TPU v7x, 32 devices: a whole 2x2x4 slice. The times are simulated.
32 devices in a mesh: ep: 4 (over y, x), tp: 8 (over z, core).
Axes of the slice: x: 2, y: 2, z: 4, core: 2. Of those that a mesh axis runs over, the one named last changes fastest.
Arguments:
- queries: bfloat16 [4096, 1024], P('ep', 'tp'), may hold values from -600 to 600
- key_rows: bfloat16 [4096, 128], P('ep'), may hold values from -6 to 6
- value_rows: bfloat16 [4096, 128], P('ep'), may hold values from -48 to 48
- sink_logits: float32 [16], P('tp'), may hold values from 2 to 6
- out_weight: bfloat16 [1024, 2048], P('tp'), may hold values from -0.1875 to 0.1875
- moe_rows: bfloat16 [1024, 2048], P(('ep', 'tp')), may hold values from -6 to 6
- moe_gain: float32 [2048], replicated, may hold values from 0.1 to 1.9
- routes: int32 [1024, 2], P(('ep', 'tp')), may hold values from 0 to 3, all different within a row; in each aligned block of 32 rows (0 to 31, 32 to 63, ...) at most 24 rows name the same one
- route_weight: float32 [1024, 2], P(('ep', 'tp')), may hold values from 0.2 to 1
- gate_weight: bfloat16 [4, 2048, 7168], P('ep', None, 'tp'), may hold values from -0.125 to 0.125
- up_weight: bfloat16 [4, 2048, 7168], P('ep', None, 'tp'), may hold values from -0.125 to 0.125
- down_weight: bfloat16 [4, 7168, 2048], P('ep', 'tp'), may hold values from -0.0625 to 0.0625
Outputs:
- mixer_out: bfloat16 [4096, 2048], P(('ep', 'tp'))
- moe_out: bfloat16 [1024, 2048], P(('ep', 'tp'))
Inputs may be any that keep to these rules, and one draw needn't show every extreme that they name: `routes`: in each aligned block of 32 rows (the rows of one device) no expert is named more than 24 times, a bound that some block reaches; each row names 2 different experts.
All inputs are finite; a program needn't handle non-finite values.
Results may differ from a plain program's by a relative error of at most 0.02.
Values may be sent and summed in bfloat16 or wider, within the bound.
A program may use at most 128 MiB of HBM per device.

v0:
```python
import jax
import jax.numpy as jnp
from jax import lax
from jax.sharding import PartitionSpec as P

HEADS = 16
KV_HEADS = 2
HEAD_DIM = 64
WINDOW = 128
TOP = 2


big_negative = -1e30
norm_eps = 1e-05


def passed_along(value, axis, steps):
    count = lax.axis_size(axis)
    initial, last = (max(0, -steps), min(count, count - steps))
    return lax.ppermute(value, axis, [(source, source + steps) for source in range(initial, last)])


def layer_normed(inputs, gain):
    values = inputs.astype(jnp.float32)
    center = values - jnp.mean(values, -1, keepdims=True)
    spread = jnp.mean(center * center, -1, keepdims=True)
    return (center * lax.rsqrt(spread + norm_eps) * gain).astype(jnp.bfloat16)


def attend(queries, key_rows, value_rows, sink_logits):
    total = queries.shape[0]
    heads_here = sink_logits.shape[0]
    blocks = total // WINDOW
    key_head = lax.axis_index("tp") * heads_here // (HEADS // KV_HEADS)
    key_own = lax.dynamic_slice_in_dim(key_rows, key_head * HEAD_DIM, HEAD_DIM, 1)
    value_own = lax.dynamic_slice_in_dim(value_rows, key_head * HEAD_DIM, HEAD_DIM, 1)
    last_rows = jnp.concatenate([key_own[total - WINDOW :], value_own[total - WINDOW :]], 1)
    earlier = passed_along(last_rows, "ep", 1)
    key_ext = jnp.concatenate([earlier[:, :HEAD_DIM], key_own], 0)
    value_ext = jnp.concatenate([earlier[:, HEAD_DIM:], value_own], 0)
    key_blocks = jnp.concatenate(
        [
            key_ext[:total].reshape(blocks, WINDOW, HEAD_DIM),
            key_ext[WINDOW:].reshape(blocks, WINDOW, HEAD_DIM),
        ],
        1,
    )
    value_blocks = jnp.concatenate(
        [
            value_ext[:total].reshape(blocks, WINDOW, HEAD_DIM),
            value_ext[WINDOW:].reshape(blocks, WINDOW, HEAD_DIM),
        ],
        1,
    )
    query_blocks = queries.reshape(blocks, WINDOW, heads_here, HEAD_DIM)
    scores = jnp.einsum(
        "nqhd,nkd->nhqk", query_blocks, key_blocks, preferred_element_type=jnp.float32
    ) * HEAD_DIM ** (-0.5)
    anchor = lax.axis_index("ep") * total
    block_base = anchor + jnp.arange(blocks, dtype=jnp.int32)[:, None, None] * WINDOW
    query_pos = block_base + jnp.arange(WINDOW, dtype=jnp.int32)[None, :, None]
    key_pos = block_base - WINDOW + jnp.arange(2 * WINDOW, dtype=jnp.int32)[None, None, :]
    allowed = ((key_pos <= query_pos) & (key_pos > query_pos - WINDOW) & (key_pos >= 0))[:, None]
    masked = jnp.where(allowed, scores, big_negative)
    sinks = sink_logits[None, :, None]
    row_max = jnp.maximum(jnp.max(masked, -1), sinks)
    powers = jnp.where(allowed, jnp.exp(masked - row_max[..., None]), 0.0)
    totals = jnp.sum(powers, -1) + jnp.exp(sinks - row_max)
    attn_probs = (powers / totals[..., None]).astype(jnp.bfloat16)
    attended = jnp.einsum(
        "nhqk,nkd->nqhd", attn_probs, value_blocks, preferred_element_type=jnp.float32
    )
    return attended.astype(jnp.bfloat16).reshape(total, heads_here * HEAD_DIM)


def mixer(queries, key_rows, value_rows, sink_logits, out_weight):
    attended = attend(queries, key_rows, value_rows, sink_logits)
    return lax.psum_scatter(
        jnp.dot(attended, out_weight, preferred_element_type=jnp.float32).astype(jnp.bfloat16),
        "tp",
        scatter_dimension=0,
        tiled=True,
    )


def experts(moe_rows, moe_gain, routes, route_weight, gate_weight, up_weight, down_weight):
    row_count = moe_rows.shape[0]
    width_all = moe_rows.shape[1]
    expert_count = gate_weight.shape[0] * lax.axis_size("ep")
    capacity = 3 * row_count * TOP // (2 * expert_count)
    normed = layer_normed(moe_rows, moe_gain)
    chosen = routes.reshape(-1)
    onehot = (chosen[:, None] == jnp.arange(expert_count, dtype=jnp.int32)[None, :]).astype(
        jnp.int32
    )
    earlier_count = jnp.cumsum(onehot, 0) - onehot
    slot_index = jnp.sum(earlier_count * onehot, 1)
    target = chosen * capacity + slot_index
    matches = target[None, :] == jnp.arange(expert_count * capacity, dtype=jnp.int32)[:, None]
    dispatch_map = jnp.sum(matches.reshape(expert_count * capacity, row_count, TOP), -1).astype(
        jnp.bfloat16
    )
    buffer = jnp.dot(dispatch_map, normed, preferred_element_type=jnp.float32).astype(jnp.bfloat16)
    buffer = buffer.reshape(expert_count, capacity, width_all)
    gate_mat = gate_weight[0]
    up_mat = up_weight[0]
    down_mat = down_weight[0]
    received = lax.all_to_all(buffer, "ep", split_axis=0, concat_axis=0, tiled=True)
    total = received.shape[0] * received.shape[1]
    flat_rows = received.reshape(total, width_all)
    shard_rows = lax.all_gather(flat_rows, "tp", axis=0, tiled=True)
    gate_val = jnp.dot(shard_rows, gate_mat, preferred_element_type=jnp.float32)
    up_val = jnp.dot(shard_rows, up_mat, preferred_element_type=jnp.float32)
    hidden = (jax.nn.silu(gate_val) * up_val).astype(jnp.bfloat16)
    summed = lax.psum_scatter(
        jnp.dot(hidden, down_mat, preferred_element_type=jnp.float32).astype(jnp.bfloat16),
        "tp",
        scatter_dimension=0,
        tiled=True,
    )
    results = summed.reshape(received.shape)
    returned = lax.all_to_all(results, "ep", split_axis=0, concat_axis=0, tiled=True)
    weights_flat = route_weight.reshape(-1)
    combine_map = jnp.sum(
        jnp.where(matches, weights_flat[None, :], 0.0).reshape(
            expert_count * capacity, row_count, TOP
        ),
        -1,
    )
    returned_flat = returned.reshape(expert_count * capacity, width_all).astype(jnp.float32)
    moe_out = lax.dot_general(
        combine_map, returned_flat, (((0,), (0,)), ((), ())), precision=lax.Precision.HIGHEST
    )
    return moe_out.astype(jnp.bfloat16)


def body(
    queries,
    key_rows,
    value_rows,
    sink_logits,
    out_weight,
    moe_rows,
    moe_gain,
    routes,
    route_weight,
    gate_weight,
    up_weight,
    down_weight,
):
    mixer_out = mixer(queries, key_rows, value_rows, sink_logits, out_weight)
    moe_out = experts(moe_rows, moe_gain, routes, route_weight, gate_weight, up_weight, down_weight)
    return (mixer_out, moe_out)


def solution(mesh):
    in_specs = (
        P("ep", "tp"),
        P("ep", None),
        P("ep", None),
        P("tp"),
        P("tp", None),
        P(("ep", "tp"), None),
        P(),
        P(("ep", "tp"), None),
        P(("ep", "tp"), None),
        P("ep", None, "tp"),
        P("ep", None, "tp"),
        P("ep", "tp", None),
    )
    out_specs = (P(("ep", "tp"), None), P(("ep", "tp"), None))
    return jax.shard_map(body, mesh=mesh, in_specs=in_specs, out_specs=out_specs, check_vma=False)
```

profile of v0, /device:TPU:0, one launch (start us, length us, event | category | flops | bytes accessed | tf_op | source)
XLA Modules:
  0.0 179.6 jit_solution(15246932592447311926)
XLA Ops:
  7.2 0.0 copy-start
  7.2 0.0 all-gather.2.cloned.1.call-start
  7.2 1.1 convert_reduce_fusion
  8.3 1.1 fusion.20
  9.4 0.8 copy.64
  10.2 0.1 eq.30
  10.3 0.1 fusion.33
  10.4 0.1 reduce_window_sum.11
  10.5 0.2 select_reduce_fusion.1
  10.7 0.1 reduce_sum.58
  10.8 0.1 copy.65
  10.9 0.7 multiply_add_fusion
  11.6 0.1 convert_reduce_fusion.1
  11.6 1.2 convolution_convert_fusion.1
  12.9 12.2 %all_to_all.10 = bf16[4,24,2048]{2,1,0:T(8,128)(2,1)} all-to-all(bf16[4,24,2048]{2,1,0:T(8,128)(2,1)S(1)} %bitcast.65), channel_id=1, replica_groups=mesh['ep'=4,'tp'=8] {'ep'}, dimensions={0} | all-to-all | bytes 786432 | tf_op jit(solution)/shard_map/all_to_all | solution.py:108
  25.1 0.0 all-gather.2.cloned.1.call-update
  25.1 0.0 reduce-scatter.5.cloned.1.call-start
  25.2 38.0 %all-gather.2.cloned.1.call-done = bf16[768,2048]{1,0:T(8,128)(2,1)} async-done(((bf16[96,2048]{1,0:T(8,128)(2,1)}), bf16[768,2048]{1,0:T(8,128)(2,1)}) %all-gather.2.cloned.1.call-update) | async-done | bytes 3145744 | tf_op jit(solution)/shard_map/all_gather | solution.py:111
  63.2 6.4 %fusion.2 = f32[768,896]{1,0:T(8,128)S(1)} fusion(bf16[768,2048]{1,0:T(8,128)(2,1)} %all-gather.2.cloned.1.call-done, bf16[1,2048,896]{2,1,0:T(8,128)(2,1)} %param.22), kind=kOutput, calls=%fused_computation.3 | convolution fusion | flops 2818572288 | bytes 9568256 | tf_op jit(solution)/shard_map/dot_general | solution.py:113
  69.6 11.8 %fusion.6 = bf16[768,2048]{1,0:T(8,128)(2,1)} fusion(bf16[1,896,2048]{2,1,0:T(8,128)(2,1)} %param.23, f32[768,896]{1,0:T(8,128)S(1)} %fusion.2, bf16[768,2048]{1,0:T(8,128)(2,1)} %all-gather.2.cloned.1.call-done, bf16[1,2048,896]{2,1,0:T(8,128)(2,1)} %param.21), kind=kOutput, calls=%fused_computation.7 | convolution fusion | flops 5642846208 | bytes 16384000 | tf_op jit(solution)/shard_map/dot_general | solution.py:116
  81.4 0.0 copy-start.2
  81.4 0.0 copy-start.1
  81.4 0.0 copy-start.3
  81.5 0.0 reduce-scatter.5.cloned.1.call-update
  81.5 0.0 reduce-scatter.3.cloned.1.call-start
  81.5 0.8 copy-done.2
  82.4 0.1 dynamic-slice
  82.5 0.0 copy-done.1
  82.5 0.1 dynamic-slice.1
  82.6 0.1 pad_maximum_fusion.2
  82.7 3.4 %collective-permute-start = (bf16[128,128]{1,0:T(8,128)(2,1)S(1)}, bf16[128,128]{1,0:T(8,128)(2,1)S(1)}, u32[]{:S(2)}, u32[]{:S(2)}) collective-permute-start(bf16[128,128]{1,0:T(8,128)(2,1)S(1)} %pad_maximum_fusion.2), channel_id=1, source_target_pairs={{0,8},{8,16},{16,24},{1,9},{9,17},{17,25},{2,10},{10,18},{18,26},{... | collective-permute-start | bytes 98312 | tf_op jit(solution)/shard_map/ppermute | solution.py:20
  86.1 0.1 broadcast_compare_fusion
  86.1 0.1 iota_add_fusion
  86.2 0.1 iota_add_fusion.1
  86.3 0.7 and_and_fusion
  87.0 0.2 constant_dynamic-slice_fusion
  87.2 0.1 copy.59
  87.4 0.1 copy.55
  87.5 0.0 copy-done.3
  87.5 0.2 reshape.202
  87.8 0.0 copy-start.4
  87.8 0.0 collective-permute-done
  87.8 0.1 fusion.41
  87.9 0.1 pad_maximum_fusion.1
  87.9 0.1 copy.54
  88.1 0.1 pad_maximum_fusion
  88.2 0.1 copy.58
  88.3 0.6 fusion.11
  88.9 0.0 copy-done.4
  88.9 0.1 broadcast_maximum_fusion
  88.9 0.6 fusion.12
  89.5 0.1 exponential_add_fusion
  89.6 0.7 fusion.13
  90.3 0.2 copy.63
  90.5 0.0 copy-done
  90.5 3.2 %convolution_convert_fusion = bf16[1024,2048]{1,0:T(8,128)(2,1)} fusion(bf16[128,2048]{1,0:T(8,128)(2,1)S(1)} %copy-done, bf16[16,8,8,128]{3,2,1,0:T(8,128)(2,1)S(1)} %bitcast.62), kind=kOutput, calls=%fused_computation | convolution fusion | flops 538968064 | bytes 4980736 | tf_op jit(solution)/shard_map/dot_general | solution.py:79
  93.7 0.0 reduce-scatter.3.cloned.1.call-update
  93.8 27.1 %reduce-scatter.5.cloned.1.call-done = bf16[96,2048]{1,0:T(8,128)(2,1)} async-done(((bf16[768,2048]{1,0:T(8,128)(2,1)}), bf16[96,2048]{1,0:T(8,128)(2,1)}) %reduce-scatter.5.cloned.1.call-update) | async-done | bytes 393232 | tf_op jit(solution)/shard_map/reduce_scatter | solution.py:115
  120.9 3.7 %all-to-all-start.1 = ((bf16[4,24,2048]{2,1,0:T(8,128)(2,1)}), bf16[4,24,2048]{2,1,0:T(8,128)(2,1)S(1)}, u32[]{:S(2)}, u32[]{:S(2)}) async-start(bf16[4,24,2048]{2,1,0:T(8,128)(2,1)} %bitcast.68), calls=%async_computation.3 | async-start | bytes 786432 | tf_op jit(solution)/shard_map/all_to_all | solution.py:122
  124.6 0.0 copy-done.5
  124.6 0.1 select_reduce_fusion
  124.7 5.8 %all-to-all-done.1 = bf16[4,24,2048]{2,1,0:T(8,128)(2,1)S(1)} async-done(((bf16[4,24,2048]{2,1,0:T(8,128)(2,1)}), bf16[4,24,2048]{2,1,0:T(8,128)(2,1)S(1)}, u32[]{:S(2)}, u32[]{:S(2)}) %all-to-all-start.1) | async-done | bytes 393248 | tf_op jit(solution)/shard_map/all_to_all | solution.py:122
  130.4 0.9 convolution_convert_fusion.2
  131.4 41.7 %reduce-scatter.3.cloned.1.call-done = bf16[128,2048]{1,0:T(8,128)(2,1)} async-done(((bf16[1024,2048]{1,0:T(8,128)(2,1)}), bf16[128,2048]{1,0:T(8,128)(2,1)}) %reduce-scatter.3.cloned.1.call-update) | async-done | bytes 524304 | tf_op jit(solution)/shard_map/reduce_scatter | solution.py:78
  (4 shorter events, 0.0 us)
Async XLA Ops:
  7.2 83.4 %copy-start = (bf16[128,2048]{1,0:T(8,128)(2,1)S(1)}, bf16[128,2048]{1,0:T(8,128)(2,1)}, u32[]{:S(2)}) copy-start(bf16[128,2048]{1,0:T(8,128)(2,1)} %param.16) | copy-start | bytes 1572868
  7.2 56.0 %all-gather.2.cloned.1.call-start = ((), (), s32[]{:S(2)}) async-start(), calls=%async_computation.5 | async-start | bytes 3538944 | tf_op jit(solution)/shard_map/all_gather | solution.py:111
  25.1 95.8 %reduce-scatter.5.cloned.1.call-start = ((), (), s32[]{:S(2)}) async-start(), calls=%async_computation.6 | async-start | bytes 3538944 | tf_op jit(solution)/shard_map/reduce_scatter | solution.py:115
  81.4 0.9 copy-start.2
  81.4 1.0 copy-start.1
  81.4 6.1 %copy-start.3 = (bf16[1024,128]{1,0:T(8,128)(2,1)S(1)}, bf16[1024,128]{1,0:T(8,128)(2,1)}, u32[]{:S(2)}) copy-start(bf16[1024,128]{1,0:T(8,128)(2,1)} %param.12) | copy-start | bytes 786436
  81.5 91.6 %reduce-scatter.3.cloned.1.call-start = ((), (), s32[]{:S(2)}) async-start(), calls=%async_computation.4 | async-start | bytes 4718592 | tf_op jit(solution)/shard_map/reduce_scatter | solution.py:78
  82.7 5.1 %collective-permute-start = (bf16[128,128]{1,0:T(8,128)(2,1)S(1)}, bf16[128,128]{1,0:T(8,128)(2,1)S(1)}, u32[]{:S(2)}, u32[]{:S(2)}) collective-permute-start(bf16[128,128]{1,0:T(8,128)(2,1)S(1)} %pad_maximum_fusion.2), channel_id=1, source_target_pairs={{0,8},{8,16},{16,24},{1,9},{9,17},{17,25},{2,10},{10,18},{18,26},{... | collective-permute-start | bytes 98312 | tf_op jit(solution)/shard_map/ppermute | solution.py:20
  87.8 1.1 copy-start.4
  93.7 30.8 %copy-start.5 = (f32[32,2]{0,1:T(2,128)S(1)}, f32[32,2]{0,1:T(2,128)}, u32[]{:S(2)}) copy-start(f32[32,2]{0,1:T(2,128)} %param.20) | copy-start | bytes 772
  120.9 9.5 %all-to-all-start.1 = ((bf16[4,24,2048]{2,1,0:T(8,128)(2,1)}), bf16[4,24,2048]{2,1,0:T(8,128)(2,1)S(1)}, u32[]{:S(2)}, u32[]{:S(2)}) async-start(bf16[4,24,2048]{2,1,0:T(8,128)(2,1)} %bitcast.68), calls=%async_computation.3 | async-start | bytes 786432 | tf_op jit(solution)/shard_map/all_to_all | solution.py:122
Sparse Core Ops, SparseCore 0:
  25.2 37.9 all-gather.1
  81.6 39.2 reduce-scatter.4
  123.8 49.2 reduce-scatter.2
where the time goes:
time: 180 us
  waiting for transfers between devices  113 us (63%)
  matrix products  24.9 us (14%)
  between operations  14 us (8%)
  blocking collectives  12.2 us (7%)
  starting transfers between devices  7.15 us (4%)
  other arithmetic  5.28 us (3%)
  local copies, waits for them, and re-layouts  3.39 us (2%)
    reduce_scatter x1, waiting for transfers between devices, mixer(): lax.psum_scatter(jnp.dot(attended, out_weight, preferred_element_type=jnp...  41.7 us
    all_gather x1, waiting for transfers between devices, experts(): shard_rows = lax.all_gather(flat_rows, 'tp', axis=0, tiled=True)  38 us
    reduce_scatter x1, waiting for transfers between devices, experts(): lax.psum_scatter(jnp.dot(hidden, down_mat, preferred_element_type=jnp.flo...  27.1 us
    all_to_all x1, blocking collectives, experts(): lax.all_to_all(buffer, 'ep', split_axis=0, concat_axis=0, tiled=True)  12.2 us
    dot_general x1, matrix products, experts(): jnp.dot(hidden, down_mat, preferred_element_type=jnp.float32)  11.8 us
    dot_general x1, matrix products, experts(): up_val = jnp.dot(shard_rows, up_mat, preferred_element_type=jnp.float32)  6.39 us
    all_to_all x1, waiting for transfers between devices, experts(): lax.all_to_all(results, 'ep', split_axis=0, concat_axis=0, tiled=True)  5.79 us
    all_to_all x1, starting transfers between devices, experts(): lax.all_to_all(results, 'ep', split_axis=0, concat_axis=0, tiled=True)  3.65 us
  transfers between devices with their start and end apart: 5, of which 4 were waited for; matrix products, arithmetic and copies ran while one was open for 5% of the time, Pallas kernels for 0%

commit v1 on v0

--- a/solution.py
+++ b/solution.py
@@ -134,6 +134,24 @@
     return moe_out.astype(jnp.bfloat16)
 
 
+def dense_experts(moe_rows, moe_gain, routes, route_weight, gate_weight, up_weight, down_weight):
+    count = lax.axis_size("ep")
+    normed = layer_normed(moe_rows, moe_gain)
+    both = ("ep", "tp")
+    rows = lax.all_gather(normed, both, axis=0, tiled=True)
+    named = routes[:, :, None] == jnp.arange(count, dtype=jnp.int32)[None, None, :]
+    shares = jnp.sum(jnp.where(named, route_weight[:, :, None], 0.0), 1)
+    shares = lax.all_gather(shares, both, axis=0, tiled=True)
+    share = lax.dynamic_slice_in_dim(shares, lax.axis_index("ep"), 1, 1)
+    gate_val = jnp.dot(rows, gate_weight[0], preferred_element_type=jnp.float32)
+    up_val = jnp.dot(rows, up_weight[0], preferred_element_type=jnp.float32)
+    hidden = (jax.nn.silu(gate_val) * up_val).astype(jnp.bfloat16)
+    down = jnp.dot(hidden, down_weight[0], preferred_element_type=jnp.float32)
+    return lax.psum_scatter(
+        (down * share).astype(jnp.bfloat16), both, scatter_dimension=0, tiled=True
+    )
+
+
 def body(
     queries,
     key_rows,
@@ -149,7 +167,10 @@
     down_weight,
 ):
     mixer_out = mixer(queries, key_rows, value_rows, sink_logits, out_weight)
-    moe_out = experts(moe_rows, moe_gain, routes, route_weight, gate_weight, up_weight, down_weight)
+    slots = 3 * moe_rows.shape[0] * TOP // 2
+    sparse = slots * lax.axis_size("tp") < moe_rows.shape[0] * lax.axis_size("tp") * lax.axis_size("ep") // 2
+    layer = experts if sparse else dense_experts
+    moe_out = layer(moe_rows, moe_gain, routes, route_weight, gate_weight, up_weight, down_weight)
     return (mixer_out, moe_out)
 
 

time: 180 us -> 266 us (1.48)
  waiting for transfers between devices: 113 us -> 168 us
  blocking collectives: 12.2 us -> 42.2 us
    reduce_scatter x1, waiting for transfers between devices: 27.1 us -> 143 us  [dense_experts(): lax.psum_scatter((down * share).astype(jnp.bfloat16), both, scatter_dimen...]
    all_gather x0 -> x1, blocking collectives: none -> 42.2 us  [dense_experts(): shares = lax.all_gather(shares, both, axis=0, tiled=True)]
    reduce_scatter x1, waiting for transfers between devices: 41.7 us -> 0.03 us  [mixer(): lax.psum_scatter(jnp.dot(attended, out_weight, preferred_element_type=jnp...]
    all_gather x1, waiting for transfers between devices: 38 us -> 25.5 us  [dense_experts(): rows = lax.all_gather(normed, both, axis=0, tiled=True)]
    all_to_all x1 -> x0, blocking collectives: 12.2 us -> none  [experts(): lax.all_to_all(buffer, 'ep', split_axis=0, concat_axis=0, tiled=True)]
    all_to_all x1 -> x0, waiting for transfers between devices: 5.79 us -> none  [experts(): lax.all_to_all(results, 'ep', split_axis=0, concat_axis=0, tiled=True)]
    all_to_all x1 -> x0, starting transfers between devices: 3.65 us -> none  [experts(): lax.all_to_all(results, 'ep', split_axis=0, concat_axis=0, tiled=True)]
    dot_general x4 -> x3, matrix products: 20.4 us -> 18.3 us  [the longest x1 7.49 us: dense_experts(): up_val = jnp.dot(rows, up_weight[0], preferred_element_type=jnp.float32)]
  transfers between devices with their start and end apart: 5 -> 4, of which waited for: 4 -> 2; matrix products, arithmetic and copies ran while one was open for 5% -> 11% of each run, Pallas kernels for 0% -> 0%
where the time goes in v1:
time: 266 us
  waiting for transfers between devices  168 us (63%)
  blocking collectives  42.2 us (16%)
  matrix products  22.9 us (9%)
  between operations  15.7 us (6%)
  other arithmetic  5.77 us (2%)
  local copies, waits for them, and re-layouts  5.72 us (2%)
  starting transfers between devices  5 us (2%)
    reduce_scatter x1, waiting for transfers between devices, dense_experts(): lax.psum_scatter((down * share).astype(jnp.bfloat16), both, scatter_dimen...  143 us
    all_gather x1, blocking collectives, dense_experts(): shares = lax.all_gather(shares, both, axis=0, tiled=True)  42.2 us
    all_gather x1, waiting for transfers between devices, dense_experts(): rows = lax.all_gather(normed, both, axis=0, tiled=True)  25.5 us
    dot_general x1, matrix products, dense_experts(): up_val = jnp.dot(rows, up_weight[0], preferred_element_type=jnp.float32)  7.49 us
    dot_general x1, matrix products, dense_experts(): down = jnp.dot(hidden, down_weight[0], preferred_element_type=jnp.float32)  6.08 us
  transfers between devices with their start and end apart: 4, of which 2 were waited for; matrix products, arithmetic and copies ran while one was open for 11% of the time, Pallas kernels for 0%

profile of v1, /device:TPU:0, one launch (start us, length us, event | category | flops | bytes accessed | tf_op | source)
XLA Modules:
  0.0 265.6 jit_solution(14966716993027986457)
XLA Ops:
  8.0 0.0 copy-start
  8.0 0.0 all-gather.3.cloned.1.call-start
  8.1 1.1 convert_reduce_fusion
  9.1 1.1 fusion.14
  10.3 1.7 fusion.16
  11.9 0.0 all-gather.3.cloned.1.call-update
  12.0 0.0 reduce-scatter.3.cloned.1.call-start
  12.0 0.8 dynamic-slice
  12.9 0.8 dynamic-slice.1
  13.7 0.1 pad_maximum_fusion.2
  13.8 4.9 %collective-permute-start = (bf16[128,128]{1,0:T(8,128)(2,1)S(1)}, bf16[128,128]{1,0:T(8,128)(2,1)S(1)}, u32[]{:S(2)}, u32[]{:S(2)}) collective-permute-start(bf16[128,128]{1,0:T(8,128)(2,1)S(1)} %pad_maximum_fusion.2), channel_id=1, source_target_pairs={{0,8},{8,16},{16,24},{1,9},{9,17},{17,25},{2,10},{10,18},{18,26},{... | collective-permute-start | bytes 98312 | tf_op jit(solution)/shard_map/ppermute | solution.py:20
  18.7 0.1 broadcast_compare_fusion
  18.8 0.1 iota_add_fusion
  18.9 0.1 iota_add_fusion.1
  19.0 0.7 and_and_fusion
  19.7 1.2 constant_dynamic-slice_fusion.1
  20.9 0.0 copy-start.1
  20.9 0.1 copy.55
  21.1 0.1 copy.51
  21.2 1.2 reshape.156
  22.4 0.0 collective-permute-done
  22.4 0.1 fusion.28
  22.5 0.1 pad_maximum_fusion.1
  22.6 0.1 copy.50
  22.7 0.1 pad_maximum_fusion
  22.8 0.1 copy.54
  22.9 0.6 fusion.7
  23.5 0.0 copy-done.1
  23.5 0.1 broadcast_maximum_fusion
  23.6 0.6 fusion.8
  24.2 0.1 exponential_add_fusion
  24.3 0.7 fusion.9
  25.0 0.2 copy.59
  25.2 0.0 copy-done
  25.2 3.2 %convolution_convert_fusion = bf16[1024,2048]{1,0:T(8,128)(2,1)} fusion(bf16[128,2048]{1,0:T(8,128)(2,1)S(1)} %copy-done, bf16[16,8,8,128]{3,2,1,0:T(8,128)(2,1)S(1)} %bitcast.57), kind=kOutput, calls=%fused_computation.1 | convolution fusion | flops 538968064 | bytes 4980736 | tf_op jit(solution)/shard_map/dot_general | solution.py:79
  28.4 0.0 copy-start.2
  28.4 0.0 copy-start.3
  28.4 0.0 reduce-scatter.3.cloned.1.call-update
  28.4 0.0 reduce-scatter.5.cloned.1.call-start
  28.5 0.6 copy-done.2
  29.1 0.0 copy-done.3
  29.1 42.2 %all-gather = f32[32,32,4]{1,2,0:T(4,128)S(1)} all-gather(f32[1,32,4]{1,2,0:T(4,128)S(1)} %bitcast.60), channel_id=1, replica_groups=mesh['ep'=4,'tp'=8] {'ep','tp'}, dimensions={0}, use_global_device_ids=true | all-gather | bytes 16896 | tf_op jit(solution)/shard_map/all_gather | solution.py:144
  71.3 0.1 reshape.153
  71.4 25.5 %all-gather.3.cloned.1.call-done = bf16[1024,2048]{1,0:T(8,128)(2,1)} async-done(((bf16[32,2048]{1,0:T(8,128)(2,1)}), bf16[1024,2048]{1,0:T(8,128)(2,1)}) %all-gather.3.cloned.1.call-update) | async-done | bytes 4194320 | tf_op jit(solution)/shard_map/all_gather | solution.py:141
  97.0 0.0 copy-start.4
  97.0 0.0 copy-start.5
  97.0 7.5 %fusion.1 = f32[1024,896]{1,0:T(8,128)S(1)} fusion(bf16[1024,2048]{1,0:T(8,128)(2,1)} %all-gather.3.cloned.1.call-done, bf16[1,2048,896]{2,1,0:T(8,128)(2,1)} %param.22), kind=kOutput, calls=%fused_computation.3 | convolution fusion | flops 3758096384 | bytes 11534336 | tf_op jit(solution)/shard_map/dot_general | solution.py:147
  104.5 0.0 copy-done.4
  104.5 0.0 copy-done.5
  104.5 0.0 copy-start.6
  104.5 4.8 %multiply_convert_fusion.1 = bf16[1024,896]{1,0:T(8,128)(2,1)S(1)} fusion(f32[1024,896]{1,0:T(8,128)S(1)} %fusion.1, bf16[1024,2048]{1,0:T(8,128)(2,1)S(1)} %copy-done.4, bf16[1,2048,896]{2,1,0:T(8,128)(2,1)S(1)} %copy-done.5), kind=kOutput, calls=%fused_computation.7 | convolution fusion | flops 3763601408 | bytes 13369344 | tf_op jit(solution)/shard_map/dot_general | solution.py:146
  109.3 0.0 copy-done.6
  109.3 6.1 %multiply_convert_fusion = bf16[1024,2048]{1,0:T(8,128)(2,1)} fusion(bf16[1024,896]{1,0:T(8,128)(2,1)S(1)} %multiply_convert_fusion.1, f32[1024]{0:T(1024)S(1)} %bitcast.61, bf16[1,896,2048]{2,1,0:T(8,128)(2,1)S(1)} %copy-done.6), kind=kOutput, calls=%fused_computation | convolution fusion | flops 3762290688 | bytes 9703424 | tf_op jit(solution)/shard_map/dot_general | solution.py:149
  115.4 0.0 reduce-scatter.5.cloned.1.call-update
  115.4 0.0 reduce-scatter.3.cloned.1.call-done
  115.4 142.8 %reduce-scatter.5.cloned.1.call-done = bf16[32,2048]{1,0:T(8,128)(2,1)} async-done(((bf16[1024,2048]{1,0:T(8,128)(2,1)}), bf16[32,2048]{1,0:T(8,128)(2,1)}) %reduce-scatter.5.cloned.1.call-update) | async-done | bytes 131088 | tf_op jit(solution)/shard_map/reduce_scatter | solution.py:150
  (6 shorter events, 0.0 us)
Async XLA Ops:
  8.0 17.2 %copy-start = (bf16[128,2048]{1,0:T(8,128)(2,1)S(1)}, bf16[128,2048]{1,0:T(8,128)(2,1)}, u32[]{:S(2)}) copy-start(bf16[128,2048]{1,0:T(8,128)(2,1)} %param.16) | copy-start | bytes 1572868
  8.0 89.0 %all-gather.3.cloned.1.call-start = ((), (), s32[]{:S(2)}) async-start(), calls=%async_computation.3 | async-start | bytes 4325376 | tf_op jit(solution)/shard_map/all_gather | solution.py:141
  12.0 103.4 %reduce-scatter.3.cloned.1.call-start = ((), (), s32[]{:S(2)}) async-start(), calls=%async_computation.2 | async-start | bytes 4718592 | tf_op jit(solution)/shard_map/reduce_scatter | solution.py:78
  13.8 8.6 %collective-permute-start = (bf16[128,128]{1,0:T(8,128)(2,1)S(1)}, bf16[128,128]{1,0:T(8,128)(2,1)S(1)}, u32[]{:S(2)}, u32[]{:S(2)}) collective-permute-start(bf16[128,128]{1,0:T(8,128)(2,1)S(1)} %pad_maximum_fusion.2), channel_id=1, source_target_pairs={{0,8},{8,16},{16,24},{1,9},{9,17},{17,25},{2,10},{10,18},{18,26},{... | collective-permute-start | bytes 98312 | tf_op jit(solution)/shard_map/ppermute | solution.py:20
  20.9 2.6 copy-start.1
  28.4 0.7 copy-start.2
  28.4 0.7 copy-start.3
  28.4 229.8 %reduce-scatter.5.cloned.1.call-start = ((), (), s32[]{:S(2)}) async-start(), calls=%async_computation.4 | async-start | bytes 4325376 | tf_op jit(solution)/shard_map/reduce_scatter | solution.py:150
  97.0 7.5 %copy-start.4 = (bf16[1024,2048]{1,0:T(8,128)(2,1)S(1)}, bf16[1024,2048]{1,0:T(8,128)(2,1)}, u32[]{:S(2)}) copy-start(bf16[1024,2048]{1,0:T(8,128)(2,1)} %all-gather.3.cloned.1.call-done) | copy-start | bytes 12582916
  97.0 7.5 %copy-start.5 = (bf16[1,2048,896]{2,1,0:T(8,128)(2,1)S(1)}, bf16[1,2048,896]{2,1,0:T(8,128)(2,1)}, u32[]{:S(2)}) copy-start(bf16[1,2048,896]{2,1,0:T(8,128)(2,1)} %param.21) | copy-start | bytes 11010052
  104.5 4.8 %copy-start.6 = (bf16[1,896,2048]{2,1,0:T(8,128)(2,1)S(1)}, bf16[1,896,2048]{2,1,0:T(8,128)(2,1)}, u32[]{:S(2)}) copy-start(bf16[1,896,2048]{2,1,0:T(8,128)(2,1)} %param.23) | copy-start | bytes 11010052
Sparse Core Ops, SparseCore 0:
  12.4 84.5 all-gather.2
Sparse Core Ops, SparseCore 1:
  28.5 64.4 reduce-scatter.2
  115.5 142.7 reduce-scatter.4

commit v2 on v0

--- a/solution.py
+++ b/solution.py
@@ -1,7 +1,13 @@
+import functools
+
 import jax
 import jax.numpy as jnp
 from jax import lax
+from jax.experimental import pallas as pl
+from jax.experimental.pallas import tpu as pltpu
 from jax.sharding import PartitionSpec as P
+
+MESH = pl.DeviceIdType.MESH
 
 HEADS = 16
 KV_HEADS = 2
@@ -134,6 +140,576 @@
     return moe_out.astype(jnp.bfloat16)
 
 
+def fused_kernel(
+    groups,
+    ranks,
+    q_ref,
+    key_ref,
+    value_ref,
+    tile_ref,
+    rows_ref,
+    gain_ref,
+    ow_hbm,
+    gate_hbm,
+    up_hbm,
+    down_hbm,
+    mix_ref,
+    moe_ref,
+    x_buf,
+    p_buf,
+    r1_buf,
+    r2_buf,
+    r3_buf,
+    ru_buf,
+    rd_buf,
+    w_buf,
+    qb_buf,
+    tiles,
+    halo,
+    kdup,
+    vdup,
+    att,
+    gate_w,
+    up_w,
+    down_w,
+    load_sem,
+    tile_ss,
+    tile_rs,
+    q_ss,
+    q_rs,
+    halo_ss,
+    halo_rs,
+    up_ss,
+    up_rs,
+    dn_ss,
+    dn_rs,
+    pa_ss,
+    pa_rs,
+    x1_ss,
+    x1_rs,
+    x2_ss,
+    x2_rs,
+    wu_ss,
+    wu_rs,
+    wd_ss,
+    wd_rs,
+    wp_ss,
+    wp_rs,
+    s1_ss,
+    s1_rs,
+    s2_ss,
+    s2_rs,
+    s3_ss,
+    s3_rs,
+    ru_ss,
+    ru_rs,
+    rd_ss,
+    rd_rs,
+):
+    chips = ranks // 2
+    total = groups * ranks
+    e, t = lax.axis_index("ep"), lax.axis_index("tp")
+    z, c = lax.div(t, 2), lax.rem(t, 2)
+    y, x = lax.div(e, 2), lax.rem(e, 2)
+    me = e * ranks + t
+    ex, ey, e3 = e + 1 - 2 * x, e + 2 - 4 * y, 3 - e
+    e1 = ex * (1 - c) + ey * c
+    e2 = ey * (1 - c) + ex * c
+    other = t + 1 - 2 * c
+    oc = 1 - c
+    columns = (e, e1, e2, e3)
+    pending = []
+
+    def remote(src, dst, ss, rs, to):
+        return pltpu.make_async_remote_copy(
+            src_ref=src, dst_ref=dst, send_sem=ss, recv_sem=rs, device_id=to, device_id_type=MESH
+        )
+
+    def send(src, dst, ss, rs, to, when=None):
+        copy = remote(src, dst, ss, rs, to)
+        pending.append((when, copy))
+        if when is None:
+            copy.start()
+        else:
+            pl.when(when)(copy.start)
+
+    def received(dst, ss, rs):
+        remote(dst, dst, ss, rs, (e, other)).wait_recv()
+
+    loads = [
+        pltpu.make_async_copy(ow_hbm, w_buf.at[t], load_sem.at[0]),
+        pltpu.make_async_copy(gate_hbm.at[0], gate_w, load_sem.at[1]),
+        pltpu.make_async_copy(up_hbm.at[0], up_w, load_sem.at[2]),
+        pltpu.make_async_copy(down_hbm.at[0], down_w, load_sem.at[3]),
+    ]
+    for load in loads:
+        load.start()
+
+    barrier = pltpu.get_barrier_semaphore()
+
+    @pl.loop(1, total)
+    def _(j):
+        to = lax.rem(me + j, total)
+        pl.semaphore_signal(
+            barrier,
+            inc=1,
+            device_id=(lax.div(to, ranks), lax.rem(to, ranks)),
+            device_id_type=MESH,
+        )
+
+    values = rows_ref[...].astype(jnp.float32)
+    center = values - jnp.mean(values, -1, keepdims=True)
+    spread = jnp.mean(center * center, -1, keepdims=True)
+    x_buf[e, z, c] = (center * lax.rsqrt(spread + norm_eps) * gain_ref[...]).astype(jnp.bfloat16)
+    tiles[me] = tile_ref[...]
+    qb_buf[t] = q_ref[pl.ds(pl.multiple_of(t * WINDOW, WINDOW), WINDOW), :]
+
+    pl.semaphore_wait(barrier, total - 1)
+
+    def spread_block(zz, up, down, when):
+        block = x_buf.at[e, zz, c]
+        if up:
+            ok = z < chips - 1
+            ok = ok if when is None else ok & when
+            send(block, block, up_ss.at[zz], up_rs.at[zz], (e, t + 2), ok)
+        if down:
+            ok = z > 0
+            ok = ok if when is None else ok & when
+            send(block, block, dn_ss.at[zz], dn_rs.at[zz], (e, t - 2), ok)
+        send(block, block, x1_ss.at[zz], x1_rs.at[zz], (e1, t), when)
+        send(block, block, x2_ss.at[zz], x2_rs.at[zz], (e2, t), when)
+        send(block, block, pa_ss.at[zz], pa_rs.at[zz], (e, other), when)
+
+    spread_block(z, True, True, None)
+
+    @pl.loop(1, ranks)
+    def _(j):
+        tt = lax.rem(t + j, ranks)
+        remote(
+            q_ref.at[pl.ds(pl.multiple_of(tt * WINDOW, WINDOW), WINDOW), :],
+            qb_buf.at[t],
+            q_ss.at[j],
+            q_rs.at[j],
+            (e, tt),
+        ).start()
+
+    @pl.loop(1, total)
+    def _(j):
+        to = lax.rem(me + j, total)
+        remote(
+            tile_ref,
+            tiles.at[me],
+            tile_ss.at[j],
+            tile_rs.at[j],
+            (lax.div(to, ranks), lax.rem(to, ranks)),
+        ).start()
+
+    last = key_ref.shape[0] - WINDOW
+    gives = (t == 0) & (e < groups - 1)
+    takes = (t == 0) & (e > 0)
+    for i, source in enumerate((key_ref, value_ref)):
+        send(
+            source.at[pl.ds(last, WINDOW), :],
+            halo.at[i],
+            halo_ss.at[i],
+            halo_rs.at[i],
+            (lax.rem(e + 1, groups), t),
+            gives,
+        )
+
+    def from_first(k):
+        sides = ((z, None),) if k == 0 else ((z - k, z >= k), (z + k, z + k < chips))
+        for zz, when in sides:
+            safe = jnp.clip(zz, 0, chips - 1)
+            block = x_buf.at[e1, safe, c]
+            wait = functools.partial(received, block, x1_ss.at[safe], x1_rs.at[safe])
+            wait() if when is None else pl.when(when)(wait)
+            slot = chips + safe
+            send(block, block, x2_ss.at[slot], x2_rs.at[slot], (e2, t), when)
+            send(block, block, pa_ss.at[slot], pa_rs.at[slot], (e, other), when)
+
+    for k in range(1, chips):
+        below, has_below = jnp.maximum(z - k, 0), z >= k
+        above, has_above = jnp.minimum(z + k, chips - 1), z + k < chips
+
+        @pl.when(has_below)
+        def _():
+            received(x_buf.at[e, below, c], up_ss.at[below], up_rs.at[below])
+
+        spread_block(below, True, False, has_below)
+
+        @pl.when(has_above)
+        def _():
+            received(x_buf.at[e, above, c], dn_ss.at[above], dn_rs.at[above])
+
+        spread_block(above, False, True, has_above)
+        from_first(k - 1)
+    from_first(chips - 1)
+
+    def spread_weight(zz, up, down, when):
+        block = w_buf.at[zz * 2 + c]
+        if up:
+            ok = z < chips - 1
+            ok = ok if when is None else ok & when
+            send(block, block, wu_ss.at[zz], wu_rs.at[zz], (e, t + 2), ok)
+        if down:
+            ok = z > 0
+            ok = ok if when is None else ok & when
+            send(block, block, wd_ss.at[zz], wd_rs.at[zz], (e, t - 2), ok)
+        send(block, block, wp_ss.at[zz], wp_rs.at[zz], (e, other), when)
+
+    def pass_weight(k):
+        below, has_below = jnp.maximum(z - k, 0), z >= k
+        above, has_above = jnp.minimum(z + k, chips - 1), z + k < chips
+
+        @pl.when(has_below)
+        def _():
+            received(w_buf.at[below * 2 + c], wu_ss.at[below], wu_rs.at[below])
+
+        spread_weight(below, True, False, has_below)
+
+        @pl.when(has_above)
+        def _():
+            received(w_buf.at[above * 2 + c], wd_ss.at[above], wd_rs.at[above])
+
+        spread_weight(above, False, True, has_above)
+
+    loads[0].wait()
+    spread_weight(z, True, True, None)
+
+    @pl.loop(1, total)
+    def _(j):
+        source = lax.rem(me + total - j, total)
+        received(tiles.at[source], tile_ss.at[j], tile_rs.at[j])
+
+    @pl.loop(1, ranks)
+    def _(j):
+        source = lax.rem(t + ranks - j, ranks)
+        received(qb_buf.at[source], q_ss.at[j], q_rs.at[j])
+
+    lanes = lax.broadcasted_iota(jnp.int32, (WINDOW, 128), 1)
+    low = lanes < HEAD_DIM
+
+    def doubled(part, rows, out):
+        wide = rows.astype(jnp.float32)
+        turned = pltpu.roll(wide, HEAD_DIM, 1)
+        place = pl.ds(part * WINDOW, WINDOW)
+        out[0, place, :] = jnp.where(low, wide, turned).astype(jnp.bfloat16)
+        out[1, place, :] = jnp.where(low, turned, wide).astype(jnp.bfloat16)
+
+    for i, (source, out) in enumerate(((key_ref, kdup), (value_ref, vdup))):
+        doubled(1, source[pl.ds(pl.multiple_of(t * WINDOW, WINDOW), WINDOW), :], out)
+
+        @pl.when(t > 0)
+        def _():
+            before = jnp.maximum(t - 1, 0) * WINDOW
+            doubled(0, source[pl.ds(pl.multiple_of(before, WINDOW), WINDOW), :], out)
+
+        @pl.when(takes)
+        def _():
+            received(halo.at[i], halo_ss.at[i], halo_rs.at[i])
+            doubled(0, halo[i], out)
+
+        @pl.when(me == 0)
+        def _():
+            doubled(0, jnp.zeros((WINDOW, 128), jnp.bfloat16), out)
+
+    query_pos = lax.broadcasted_iota(jnp.int32, (WINDOW, 2 * WINDOW), 0) + WINDOW
+    key_pos = lax.broadcasted_iota(jnp.int32, (WINDOW, 2 * WINDOW), 1)
+    first = jnp.where(me == 0, WINDOW, 0)
+    allowed = (key_pos <= query_pos) & (key_pos > query_pos - WINDOW) & (key_pos >= first)
+
+    @pl.loop(0, ranks)
+    def _(j):
+        pair = qb_buf[j]
+        kept = lax.div(j * KV_HEADS, ranks)
+        keys, vals = kdup[kept], vdup[kept]
+        outs = []
+        for i in range(2):
+            mine = low if i == 0 else jnp.logical_not(low)
+            query = jnp.where(mine, pair, jnp.zeros_like(pair))
+            scores = lax.dot_general(
+                query, keys, (((1,), (1,)), ((), ())), preferred_element_type=jnp.float32
+            ) * HEAD_DIM ** (-0.5)
+            masked = jnp.where(allowed, scores, big_negative)
+            sink = tiles[e * ranks + j, groups : groups + 1, i : i + 1]
+            row_max = jnp.maximum(jnp.max(masked, -1, keepdims=True), sink)
+            powers = jnp.exp(masked - row_max)
+            totals = jnp.sum(powers, -1, keepdims=True) + jnp.exp(sink - row_max)
+            probs = (powers / totals).astype(jnp.bfloat16)
+            outs.append(jnp.dot(probs, vals, preferred_element_type=jnp.float32))
+        att[:, pl.ds(pl.multiple_of(j * 128, 128), 128)] = jnp.where(low, outs[0], outs[1]).astype(
+            jnp.bfloat16
+        )
+
+    for load in loads[1:]:
+        load.wait()
+
+    row_count = rows_ref.shape[0]
+    width = rows_ref.shape[1]
+    diagonal = lax.broadcasted_iota(jnp.int32, (row_count, 128), 0) == lax.broadcasted_iota(
+        jnp.int32, (row_count, 128), 1
+    )
+
+    def column_of(i):
+        xi = x + lax.rem(i, 2) * (1 - 2 * x)
+        yi = y + lax.div(i, 2) * (1 - 2 * y)
+        return yi * 2 + xi
+
+    def partner_column(slot_column, slot):
+        for zz in range(chips):
+            where = slot * chips + zz
+            received(x_buf.at[slot_column, zz, oc], pa_ss.at[where], pa_rs.at[where])
+
+    def from_second(slot):
+        column = e2 if slot == 0 else e3
+        for zz in range(chips):
+            where = slot * chips + zz
+            block = x_buf.at[column, zz, c]
+            received(block, x2_ss.at[where], x2_rs.at[where])
+            to = (2 + slot) * chips + zz
+            remote(block, block, pa_ss.at[to], pa_rs.at[to], (e, other)).start()
+
+    def fold(i):
+        column = column_of(i)
+        received(r1_buf.at[i], s1_ss.at[i], s1_rs.at[i])
+        for zz in range(chips):
+            p_buf[column, zz, c] = (
+                p_buf[column, zz, c].astype(jnp.float32) + r1_buf[i, zz].astype(jnp.float32)
+            ).astype(jnp.bfloat16)
+
+        @pl.when((column == e2) | (column == e3))
+        def _():
+            slot = jnp.where(column == e3, 1, 0)
+            remote(
+                p_buf.at[column, :, c], r2_buf.at[slot], s2_ss.at[slot], s2_rs.at[slot], (e2, t)
+            ).start()
+
+    @pl.loop(0, groups)
+    def _(i):
+        column = column_of(i)
+
+        @pl.when(i == 0)
+        def _():
+            partner_column(e, 0)
+
+        @pl.when(i == 1)
+        def _():
+            from_second(0)
+            partner_column(e1, 2)
+            partner_column(e2, 1)
+
+        @pl.when(i == 3)
+        def _():
+            from_second(1)
+            partner_column(e3, 3)
+
+        rows = x_buf[column].reshape(ranks * row_count, width)
+        gate_val = jnp.dot(rows, gate_w[...], preferred_element_type=jnp.float32)
+        up_val = jnp.dot(rows, up_w[...], preferred_element_type=jnp.float32)
+        hidden = (gate_val / (1.0 + jnp.exp(-gate_val)) * up_val).astype(jnp.bfloat16)
+        shares = []
+        for j in range(ranks):
+            line = tiles[column * ranks + j, pl.ds(e, 1), :]
+            shares.append(
+                jnp.sum(
+                    jnp.where(diagonal, jnp.broadcast_to(line, (row_count, 128)), 0.0),
+                    -1,
+                    keepdims=True,
+                )
+            )
+        share = jnp.concatenate(shares, 0)
+        down = jnp.dot(hidden, down_w[...], preferred_element_type=jnp.float32)
+        p_buf[column] = (
+            (down * share).astype(jnp.bfloat16).reshape(chips, 2, row_count, width)
+        )
+        remote(
+            p_buf.at[column, :, oc], r1_buf.at[i], s1_ss.at[i], s1_rs.at[i], (e, other)
+        ).start()
+
+        @pl.when(i > 0)
+        def _():
+            fold(i - 1)
+
+    if chips > 1:
+        pass_weight(1)
+    fold(groups - 1)
+
+    def add_in(block, extra):
+        block[...] = (block[...].astype(jnp.float32) + extra[...].astype(jnp.float32)).astype(
+            jnp.bfloat16
+        )
+
+    received(r2_buf.at[1], s2_ss.at[1], s2_rs.at[1])
+    for zz in range(chips):
+        add_in(p_buf.at[e1, zz, c], r2_buf.at[1, zz])
+    send(p_buf.at[e1, :, c], r3_buf, s3_ss.at[0], s3_rs.at[0], (e1, t))
+    received(r2_buf.at[0], s2_ss.at[0], s2_rs.at[0])
+    for zz in range(chips):
+        add_in(p_buf.at[e, zz, c], r2_buf.at[0, zz])
+    if chips > 2:
+        pass_weight(2)
+    received(r3_buf, s3_ss.at[0], s3_rs.at[0])
+    for zz in range(chips):
+        add_in(p_buf.at[e, zz, c], r3_buf.at[zz])
+
+    for k in range(chips - 1):
+        for zz, mine, inner, buf, ss, rs, to in (
+            (chips - 1 - k, z < chips - 1 - k, z > 0, ru_buf, ru_ss, ru_rs, t + 2),
+            (k, z > k, z < chips - 1, rd_buf, rd_ss, rd_rs, t - 2),
+        ):
+
+            @pl.when(mine & inner)
+            def _():
+                received(buf.at[zz], ss.at[zz], rs.at[zz])
+                add_in(p_buf.at[e, zz, c], buf.at[zz])
+
+            send(p_buf.at[e, zz, c], buf.at[zz], ss.at[zz], rs.at[zz], (e, to), mine)
+
+    for k in range(3, chips):
+        pass_weight(k)
+    for zz in range(chips):
+        received(w_buf.at[zz * 2 + oc], wp_ss.at[zz], wp_rs.at[zz])
+    mix_ref[...] = jnp.dot(
+        att[...], w_buf[...].reshape(ranks * 128, width), preferred_element_type=jnp.float32
+    ).astype(jnp.bfloat16)
+
+    @pl.when(z > 0)
+    def _():
+        received(ru_buf.at[z], ru_ss.at[z], ru_rs.at[z])
+        add_in(p_buf.at[e, z, c], ru_buf.at[z])
+
+    @pl.when(z < chips - 1)
+    def _():
+        received(rd_buf.at[z], rd_ss.at[z], rd_rs.at[z])
+        add_in(p_buf.at[e, z, c], rd_buf.at[z])
+
+    moe_ref[...] = p_buf[e, z, c]
+
+    for when, copy in pending:
+        copy.wait_send() if when is None else pl.when(when)(copy.wait_send)
+    for slot in range(2 * chips, 4 * chips):
+        block = x_buf.at[e, z, c]
+        remote(block, block, pa_ss.at[slot], pa_rs.at[slot], (e, other)).wait_send()
+
+    @pl.loop(0, groups)
+    def _(i):
+        remote(
+            p_buf.at[e, :, oc], r1_buf.at[i], s1_ss.at[i], s1_rs.at[i], (e, other)
+        ).wait_send()
+
+    for slot in range(2):
+        remote(
+            p_buf.at[e2, :, c], r2_buf.at[slot], s2_ss.at[slot], s2_rs.at[slot], (e2, t)
+        ).wait_send()
+
+    @pl.loop(1, ranks)
+    def _(j):
+        remote(qb_buf.at[t], qb_buf.at[t], q_ss.at[j], q_rs.at[j], (e, other)).wait_send()
+
+    @pl.loop(1, total)
+    def _(j):
+        remote(tile_ref, tiles.at[me], tile_ss.at[j], tile_rs.at[j], (e, other)).wait_send()
+
+
+def fused(
+    queries,
+    key_rows,
+    value_rows,
+    sink_logits,
+    out_weight,
+    moe_rows,
+    moe_gain,
+    routes,
+    route_weight,
+    gate_weight,
+    up_weight,
+    down_weight,
+):
+    groups, ranks = lax.axis_size("ep"), lax.axis_size("tp")
+    chips, total = ranks // 2, groups * ranks
+    row_count, width = moe_rows.shape
+    units = gate_weight.shape[2]
+    chosen, weights = routes.T, route_weight.T
+    named = chosen[:, None, :] == jnp.arange(groups, dtype=jnp.int32)[None, :, None]
+    shares = jnp.sum(jnp.where(named, weights[:, None, :], 0.0), 0)
+    tile_rows = -(-(groups + 1) // 8) * 8
+    shares = jnp.pad(shares, ((0, tile_rows - groups), (0, 128 - row_count)))
+    sinks = jnp.pad(
+        sink_logits[None, :], ((groups, tile_rows - groups - 1), (0, 128 - sink_logits.shape[0]))
+    )
+    tile = shares + sinks
+    bf16, f32 = jnp.bfloat16, jnp.float32
+    vmem = pltpu.VMEM
+    dma = pltpu.SemaphoreType.DMA
+    sems = [(4,)]
+    for count in (
+        total,
+        ranks,
+        2,
+        chips,
+        chips,
+        4 * chips,
+        chips,
+        2 * chips,
+        chips,
+        chips,
+        chips,
+        groups,
+        2,
+        1,
+        chips,
+        chips,
+    ):
+        sems += [(count,), (count,)]
+    block = (row_count, width)
+    in_vmem = pl.BlockSpec(memory_space=pltpu.VMEM)
+    in_any = pl.BlockSpec(memory_space=pl.ANY)
+    return pl.pallas_call(
+        functools.partial(fused_kernel, groups, ranks),
+        out_shape=(
+            jax.ShapeDtypeStruct((queries.shape[0] // ranks, width), bf16),
+            jax.ShapeDtypeStruct(block, bf16),
+        ),
+        in_specs=[in_vmem] * 6 + [in_any] * 4,
+        out_specs=(in_vmem, in_vmem),
+        scratch_shapes=[
+            vmem((groups, chips, 2) + block, bf16),
+            vmem((groups, chips, 2) + block, bf16),
+            vmem((groups, chips) + block, bf16),
+            vmem((2, chips) + block, bf16),
+            vmem((chips,) + block, bf16),
+            vmem((chips,) + block, bf16),
+            vmem((chips,) + block, bf16),
+            vmem((ranks,) + out_weight.shape, bf16),
+            vmem((ranks, WINDOW, 128), bf16),
+            vmem((total, tile_rows, 128), f32),
+            vmem((2, WINDOW, 128), bf16),
+            vmem((2, 2 * WINDOW, 128), bf16),
+            vmem((2, 2 * WINDOW, 128), bf16),
+            vmem((WINDOW, ranks * 128), bf16),
+            vmem((width, units), bf16),
+            vmem((width, units), bf16),
+            vmem((units, width), bf16),
+        ]
+        + [dma(shape) for shape in sems],
+        compiler_params=pltpu.CompilerParams(
+            collective_id=0, has_side_effects=True, vmem_limit_bytes=60 * 1024 * 1024
+        ),
+    )(
+        queries,
+        key_rows,
+        value_rows,
+        tile,
+        moe_rows,
+        moe_gain[None, :],
+        out_weight,
+        gate_weight,
+        up_weight,
+        down_weight,
+    )
+
+
 def body(
     queries,
     key_rows,
@@ -148,6 +724,25 @@
     up_weight,
     down_weight,
 ):
+    groups, ranks = lax.axis_size("ep"), lax.axis_size("tp")
+    fits = groups == 4 and ranks % 2 == 0 and ranks <= 8
+    fits = fits and queries.shape == (ranks * WINDOW, 2 * HEAD_DIM)
+    fits = fits and key_rows.shape[1] == 128 and moe_rows.shape[0] % 16 == 0
+    if fits:
+        return fused(
+            queries,
+            key_rows,
+            value_rows,
+            sink_logits,
+            out_weight,
+            moe_rows,
+            moe_gain,
+            routes,
+            route_weight,
+            gate_weight,
+            up_weight,
+            down_weight,
+        )
     mixer_out = mixer(queries, key_rows, value_rows, sink_logits, out_weight)
     moe_out = experts(moe_rows, moe_gain, routes, route_weight, gate_weight, up_weight, down_weight)
     return (mixer_out, moe_out)

time: 180 us -> 113 us (0.63)
  waiting for transfers between devices: 113 us -> 0 us
  Pallas kernels: 0 us -> 106 us
  matrix products: 24.9 us -> 0 us
  between operations: 14 us -> 0.64 us
  blocking collectives: 12.2 us -> 0 us
  starting transfers between devices: 7.15 us -> 0 us
  other arithmetic: 5.28 us -> 1.96 us
    pallas_call x0 -> x1, Pallas kernels: none -> 106 us  [fused(): pl.pallas_call(functools.partial(fused_kernel, groups, ranks), out_shape=...]
    reduce_scatter x2 -> x0, waiting for transfers between devices: 68.8 us -> none  [the longest x1 41.7 us: mixer(): lax.psum_scatter(jnp.dot(attended, out_weight, preferred_element_type=jnp...]
    all_gather x1 -> x0, waiting for transfers between devices: 38 us -> none  [experts(): shard_rows = lax.all_gather(flat_rows, 'tp', axis=0, tiled=True)]
    dot_general x7 -> x0, matrix products: 24.9 us -> none  [the longest x1 11.8 us: experts(): jnp.dot(hidden, down_mat, preferred_element_type=jnp.float32)]
    all_to_all x1 -> x0, blocking collectives: 12.2 us -> none  [experts(): lax.all_to_all(buffer, 'ep', split_axis=0, concat_axis=0, tiled=True)]
    all_to_all x1 -> x0, waiting for transfers between devices: 5.79 us -> none  [experts(): lax.all_to_all(results, 'ep', split_axis=0, concat_axis=0, tiled=True)]
    all_to_all x1 -> x0, starting transfers between devices: 3.65 us -> none  [experts(): lax.all_to_all(results, 'ep', split_axis=0, concat_axis=0, tiled=True)]
    ppermute x1 -> x0, starting transfers between devices: 3.38 us -> none  [passed_along(): lax.ppermute(value, axis, [(source, source + steps) for source in range(i...]
  transfers between devices with their start and end apart: 5 -> 0, of which waited for: 4 -> 0; matrix products, arithmetic and copies ran while one was open for 5% -> 0% of each run, Pallas kernels for 0% -> 0%
where the time goes in v2:
time: 113 us; the launch traced here: 112 us
  Pallas kernels  106 us (94%)
  local copies, waits for them, and re-layouts  3.45 us (3%)
  other arithmetic  1.96 us (2%)
    pallas_call x1, Pallas kernels, fused(): pl.pallas_call(functools.partial(fused_kernel, groups, ranks), out_shape=...  106 us
    unnamed x2, local copies, waits for them, and re-layouts  3.45 us

profile of v2, /device:TPU:0, one launch (start us, length us, event | category | flops | bytes accessed | tf_op | source)
XLA Modules:
  0.0 112.3 jit_solution(17919739046929266540)
XLA Ops:
  0.6 0.7 select_reduce_fusion
  1.3 1.3 %pad_add_fusion.tile_ref = f32[8,128]{1,0:T(8,128)} fusion(f32[1,2]{1,0:T(1,128)} %bitcast.7, f32[4,32]{1,0:T(4,128)S(1)} %select_reduce_fusion), kind=kLoop, calls=%fused_computation | loop fusion | flops 1024 | bytes 4616 | tf_op jit(solution)/shard_map/add | solution.py:641
  2.6 106.3 %shard_map.131 = (bf16[128,2048]{1,0:T(8,128)(2,1)}, bf16[32,2048]{1,0:T(8,128)(2,1)}) custom-call(bf16[1024,128]{1,0:T(8,128)(2,1)} %q_ref.1, bf16[1024,128]{1,0:T(8,128)(2,1)} %key_ref.1, bf16[1024,128]{1,0:T(8,128)(2,1)} %value_ref.1, f32[8,128]{1,0:T(8,128)} %pad_add_fusion.tile_ref, bf16[32,2048]{1,0:T(8,128)(2,1)} %rows_ref.1, f32[1,2048]{1,0:T(1,128)} %bitcast.4, ...), custom_call_target="tpu_custom_call" | custom-call | tf_op jit(solution)/shard_map/pallas_call | solution.py:668
  108.9 1.9 %copy.16 = bf16[128,2048]{1,0:T(8,128)(2,1)} copy(bf16[128,2048]{1,0:T(8,128)(2,1)} %get-tuple-element.4) | data formatting | bytes 1048576
  110.8 1.6 %copy.17 = bf16[32,2048]{1,0:T(8,128)(2,1)} copy(bf16[32,2048]{1,0:T(8,128)(2,1)} %get-tuple-element.5) | data formatting | bytes 262144

commit v3 on v2

--- a/solution.py
+++ b/solution.py
@@ -195,6 +195,10 @@
     wd_rs,
     wp_ss,
     wp_rs,
+    wx_ss,
+    wx_rs,
+    wq_ss,
+    wq_rs,
     s1_ss,
     s1_rs,
     s2_ss,
@@ -266,43 +270,35 @@
 
     pl.semaphore_wait(barrier, total - 1)
 
+    piece_rows = rows_ref.shape[0] // 2
+
     def spread_block(zz, up, down, when):
         block = x_buf.at[e, zz, c]
         if up:
             ok = z < chips - 1
             ok = ok if when is None else ok & when
-            send(block, block, up_ss.at[zz], up_rs.at[zz], (e, t + 2), ok)
+            for h in range(2):
+                part = block.at[pl.ds(h * piece_rows, piece_rows), :]
+                at = zz * 2 + h
+                if when is not None:
+                    wait = functools.partial(received, part, up_ss.at[at], up_rs.at[at])
+                    pl.when(when)(wait)
+                send(part, part, up_ss.at[at], up_rs.at[at], (e, t + 2), ok)
         if down:
             ok = z > 0
             ok = ok if when is None else ok & when
-            send(block, block, dn_ss.at[zz], dn_rs.at[zz], (e, t - 2), ok)
+            for h in range(2):
+                part = block.at[pl.ds(h * piece_rows, piece_rows), :]
+                at = zz * 2 + h
+                if when is not None:
+                    wait = functools.partial(received, part, dn_ss.at[at], dn_rs.at[at])
+                    pl.when(when)(wait)
+                send(part, part, dn_ss.at[at], dn_rs.at[at], (e, t - 2), ok)
         send(block, block, x1_ss.at[zz], x1_rs.at[zz], (e1, t), when)
         send(block, block, x2_ss.at[zz], x2_rs.at[zz], (e2, t), when)
         send(block, block, pa_ss.at[zz], pa_rs.at[zz], (e, other), when)
 
     spread_block(z, True, True, None)
-
-    @pl.loop(1, ranks)
-    def _(j):
-        tt = lax.rem(t + j, ranks)
-        remote(
-            q_ref.at[pl.ds(pl.multiple_of(tt * WINDOW, WINDOW), WINDOW), :],
-            qb_buf.at[t],
-            q_ss.at[j],
-            q_rs.at[j],
-            (e, tt),
-        ).start()
-
-    @pl.loop(1, total)
-    def _(j):
-        to = lax.rem(me + j, total)
-        remote(
-            tile_ref,
-            tiles.at[me],
-            tile_ss.at[j],
-            tile_rs.at[j],
-            (lax.div(to, ranks), lax.rem(to, ranks)),
-        ).start()
 
     last = key_ref.shape[0] - WINDOW
     gives = (t == 0) & (e < groups - 1)
@@ -328,119 +324,91 @@
             send(block, block, x2_ss.at[slot], x2_rs.at[slot], (e2, t), when)
             send(block, block, pa_ss.at[slot], pa_rs.at[slot], (e, other), when)
 
+    third = w_buf.shape[1] // 4
+    side = x * (1 - c) + y * c
+    carried = pl.ds(pl.multiple_of(side * third, third), 3 * third)
+    given = pl.ds(pl.multiple_of(3 * side * third, third), third)
+    taken = pl.ds(pl.multiple_of(3 * (1 - side) * third, third), third)
+
+    other_side = x * c + y * (1 - c)
+    other_carried = pl.ds(pl.multiple_of(other_side * third, third), 3 * third)
+    other_taken = pl.ds(pl.multiple_of(3 * (1 - other_side) * third, third), third)
+
+    def weight_copies(zz, up, down, when):
+        block = w_buf.at[zz * 2 + c, carried, :]
+        copies = []
+        if up:
+            ok = z < chips - 1
+            ok = ok if when is None else ok & when
+            copies.append((ok, remote(block, block, wu_ss.at[zz], wu_rs.at[zz], (e, t + 2))))
+        if down:
+            ok = z > 0
+            ok = ok if when is None else ok & when
+            copies.append((ok, remote(block, block, wd_ss.at[zz], wd_rs.at[zz], (e, t - 2))))
+        copies.append((when, remote(block, block, wp_ss.at[zz], wp_rs.at[zz], (e, other))))
+        if when is None:
+            rest = w_buf.at[zz * 2 + c, taken, :]
+            copies.append((when, remote(rest, rest, wq_ss.at[zz], wq_rs.at[zz], (e, other))))
+        else:
+            piece = w_buf.at[zz * 2 + c, given, :]
+            copies.append((when, remote(piece, piece, wx_ss.at[zz], wx_rs.at[zz], (e1, t))))
+        return copies
+
+    def spread_weight(zz, up, down, when):
+        for ok, copy in weight_copies(zz, up, down, when):
+            copy.start() if ok is None else pl.when(ok)(copy.start)
+
+    def pass_weight(k):
+        below, has_below = jnp.maximum(z - k, 0), z >= k
+        above, has_above = jnp.minimum(z + k, chips - 1), z + k < chips
+
+        @pl.when(has_below)
+        def _():
+            received(w_buf.at[below * 2 + c, carried, :], wu_ss.at[below], wu_rs.at[below])
+
+        spread_weight(below, True, False, has_below)
+
+        @pl.when(has_above)
+        def _():
+            received(w_buf.at[above * 2 + c, carried, :], wd_ss.at[above], wd_rs.at[above])
+
+        spread_weight(above, False, True, has_above)
+
     for k in range(1, chips):
         below, has_below = jnp.maximum(z - k, 0), z >= k
         above, has_above = jnp.minimum(z + k, chips - 1), z + k < chips
 
-        @pl.when(has_below)
-        def _():
-            received(x_buf.at[e, below, c], up_ss.at[below], up_rs.at[below])
-
         spread_block(below, True, False, has_below)
-
-        @pl.when(has_above)
-        def _():
-            received(x_buf.at[e, above, c], dn_ss.at[above], dn_rs.at[above])
 
         spread_block(above, False, True, has_above)
         from_first(k - 1)
     from_first(chips - 1)
 
-    def spread_weight(zz, up, down, when):
-        block = w_buf.at[zz * 2 + c]
-        if up:
-            ok = z < chips - 1
-            ok = ok if when is None else ok & when
-            send(block, block, wu_ss.at[zz], wu_rs.at[zz], (e, t + 2), ok)
-        if down:
-            ok = z > 0
-            ok = ok if when is None else ok & when
-            send(block, block, wd_ss.at[zz], wd_rs.at[zz], (e, t - 2), ok)
-        send(block, block, wp_ss.at[zz], wp_rs.at[zz], (e, other), when)
-
-    def pass_weight(k):
-        below, has_below = jnp.maximum(z - k, 0), z >= k
-        above, has_above = jnp.minimum(z + k, chips - 1), z + k < chips
-
-        @pl.when(has_below)
-        def _():
-            received(w_buf.at[below * 2 + c], wu_ss.at[below], wu_rs.at[below])
-
-        spread_weight(below, True, False, has_below)
-
-        @pl.when(has_above)
-        def _():
-            received(w_buf.at[above * 2 + c], wd_ss.at[above], wd_rs.at[above])
-
-        spread_weight(above, False, True, has_above)
+    @pl.loop(1, total)
+    def _(j):
+        to = lax.rem(me + j, total)
+        remote(
+            tile_ref,
+            tiles.at[me],
+            tile_ss.at[j],
+            tile_rs.at[j],
+            (lax.div(to, ranks), lax.rem(to, ranks)),
+        ).start()
+
+    @pl.loop(1, ranks)
+    def _(j):
+        tt = lax.rem(t + j, ranks)
+        remote(
+            q_ref.at[pl.ds(pl.multiple_of(tt * WINDOW, WINDOW), WINDOW), :],
+            qb_buf.at[t],
+            q_ss.at[j],
+            q_rs.at[j],
+            (e, tt),
+        ).start()
 
     loads[0].wait()
     spread_weight(z, True, True, None)
 
-    @pl.loop(1, total)
-    def _(j):
-        source = lax.rem(me + total - j, total)
-        received(tiles.at[source], tile_ss.at[j], tile_rs.at[j])
-
-    @pl.loop(1, ranks)
-    def _(j):
-        source = lax.rem(t + ranks - j, ranks)
-        received(qb_buf.at[source], q_ss.at[j], q_rs.at[j])
-
-    lanes = lax.broadcasted_iota(jnp.int32, (WINDOW, 128), 1)
-    low = lanes < HEAD_DIM
-
-    def doubled(part, rows, out):
-        wide = rows.astype(jnp.float32)
-        turned = pltpu.roll(wide, HEAD_DIM, 1)
-        place = pl.ds(part * WINDOW, WINDOW)
-        out[0, place, :] = jnp.where(low, wide, turned).astype(jnp.bfloat16)
-        out[1, place, :] = jnp.where(low, turned, wide).astype(jnp.bfloat16)
-
-    for i, (source, out) in enumerate(((key_ref, kdup), (value_ref, vdup))):
-        doubled(1, source[pl.ds(pl.multiple_of(t * WINDOW, WINDOW), WINDOW), :], out)
-
-        @pl.when(t > 0)
-        def _():
-            before = jnp.maximum(t - 1, 0) * WINDOW
-            doubled(0, source[pl.ds(pl.multiple_of(before, WINDOW), WINDOW), :], out)
-
-        @pl.when(takes)
-        def _():
-            received(halo.at[i], halo_ss.at[i], halo_rs.at[i])
-            doubled(0, halo[i], out)
-
-        @pl.when(me == 0)
-        def _():
-            doubled(0, jnp.zeros((WINDOW, 128), jnp.bfloat16), out)
-
-    query_pos = lax.broadcasted_iota(jnp.int32, (WINDOW, 2 * WINDOW), 0) + WINDOW
-    key_pos = lax.broadcasted_iota(jnp.int32, (WINDOW, 2 * WINDOW), 1)
-    first = jnp.where(me == 0, WINDOW, 0)
-    allowed = (key_pos <= query_pos) & (key_pos > query_pos - WINDOW) & (key_pos >= first)
-
-    @pl.loop(0, ranks)
-    def _(j):
-        pair = qb_buf[j]
-        kept = lax.div(j * KV_HEADS, ranks)
-        keys, vals = kdup[kept], vdup[kept]
-        outs = []
-        for i in range(2):
-            mine = low if i == 0 else jnp.logical_not(low)
-            query = jnp.where(mine, pair, jnp.zeros_like(pair))
-            scores = lax.dot_general(
-                query, keys, (((1,), (1,)), ((), ())), preferred_element_type=jnp.float32
-            ) * HEAD_DIM ** (-0.5)
-            masked = jnp.where(allowed, scores, big_negative)
-            sink = tiles[e * ranks + j, groups : groups + 1, i : i + 1]
-            row_max = jnp.maximum(jnp.max(masked, -1, keepdims=True), sink)
-            powers = jnp.exp(masked - row_max)
-            totals = jnp.sum(powers, -1, keepdims=True) + jnp.exp(sink - row_max)
-            probs = (powers / totals).astype(jnp.bfloat16)
-            outs.append(jnp.dot(probs, vals, preferred_element_type=jnp.float32))
-        att[:, pl.ds(pl.multiple_of(j * 128, 128), 128)] = jnp.where(low, outs[0], outs[1]).astype(
-            jnp.bfloat16
-        )
 
     for load in loads[1:]:
         load.wait()
@@ -470,6 +438,12 @@
             to = (2 + slot) * chips + zz
             remote(block, block, pa_ss.at[to], pa_rs.at[to], (e, other)).start()
 
+    far_first = []
+    for k in range(chips - 1, 0, -1):
+        far_first.append((jnp.maximum(z - k, 0), z >= k))
+        far_first.append((jnp.minimum(z + k, chips - 1), z + k < chips))
+    far_first.append((z, None))
+
     def fold(i):
         column = column_of(i)
         received(r1_buf.at[i], s1_ss.at[i], s1_rs.at[i])
@@ -481,9 +455,16 @@
         @pl.when((column == e2) | (column == e3))
         def _():
             slot = jnp.where(column == e3, 1, 0)
-            remote(
-                p_buf.at[column, :, c], r2_buf.at[slot], s2_ss.at[slot], s2_rs.at[slot], (e2, t)
-            ).start()
+            for zz, when in far_first:
+                place = slot * chips + zz
+                copy = remote(
+                    p_buf.at[column, zz, c],
+                    r2_buf.at[slot, zz],
+                    s2_ss.at[place],
+                    s2_rs.at[place],
+                    (e2, t),
+                )
+                copy.start() if when is None else pl.when(when)(copy.start)
 
     @pl.loop(0, groups)
     def _(i):
@@ -503,11 +484,29 @@
         def _():
             from_second(1)
             partner_column(e3, 3)
+
+        if chips > 1:
+
+            @pl.when(i == 2)
+            def _():
+                pass_weight(1)
 
         rows = x_buf[column].reshape(ranks * row_count, width)
         gate_val = jnp.dot(rows, gate_w[...], preferred_element_type=jnp.float32)
         up_val = jnp.dot(rows, up_w[...], preferred_element_type=jnp.float32)
         hidden = (gate_val / (1.0 + jnp.exp(-gate_val)) * up_val).astype(jnp.bfloat16)
+
+        @pl.when(i > 0)
+        def _():
+            fold(i - 1)
+
+        @pl.when(i == 0)
+        def _():
+            @pl.loop(1, total)
+            def _(j):
+                source = lax.rem(me + total - j, total)
+                received(tiles.at[source], tile_ss.at[j], tile_rs.at[j])
+
         shares = []
         for j in range(ranks):
             line = tiles[column * ranks + j, pl.ds(e, 1), :]
@@ -527,65 +526,167 @@
             p_buf.at[column, :, oc], r1_buf.at[i], s1_ss.at[i], s1_rs.at[i], (e, other)
         ).start()
 
-        @pl.when(i > 0)
-        def _():
-            fold(i - 1)
-
-    if chips > 1:
-        pass_weight(1)
     fold(groups - 1)
+    if chips > 2:
+        pass_weight(2)
+
+    @pl.loop(1, ranks)
+    def _(j):
+        source = lax.rem(t + ranks - j, ranks)
+        received(qb_buf.at[source], q_ss.at[j], q_rs.at[j])
+
+    lanes = lax.broadcasted_iota(jnp.int32, (WINDOW, 128), 1)
+    low = lanes < HEAD_DIM
+
+    def doubled(part, rows, out):
+        wide = rows.astype(jnp.float32)
+        turned = pltpu.roll(wide, HEAD_DIM, 1)
+        place = pl.ds(part * WINDOW, WINDOW)
+        out[0, place, :] = jnp.where(low, wide, turned).astype(jnp.bfloat16)
+        out[1, place, :] = jnp.where(low, turned, wide).astype(jnp.bfloat16)
+
+    for i, (source, out) in enumerate(((key_ref, kdup), (value_ref, vdup))):
+        doubled(1, source[pl.ds(pl.multiple_of(t * WINDOW, WINDOW), WINDOW), :], out)
+
+        @pl.when(t > 0)
+        def _():
+            before = jnp.maximum(t - 1, 0) * WINDOW
+            doubled(0, source[pl.ds(pl.multiple_of(before, WINDOW), WINDOW), :], out)
+
+        @pl.when(takes)
+        def _():
+            received(halo.at[i], halo_ss.at[i], halo_rs.at[i])
+            doubled(0, halo[i], out)
+
+        @pl.when(me == 0)
+        def _():
+            doubled(0, jnp.zeros((WINDOW, 128), jnp.bfloat16), out)
+
+    query_pos = lax.broadcasted_iota(jnp.int32, (WINDOW, 2 * WINDOW), 0) + WINDOW
+    key_pos = lax.broadcasted_iota(jnp.int32, (WINDOW, 2 * WINDOW), 1)
+    first = jnp.where(me == 0, WINDOW, 0)
+    allowed = (key_pos <= query_pos) & (key_pos > query_pos - WINDOW) & (key_pos >= first)
+
+    def attend_pairs(begin, end):
+        @pl.loop(begin, end)
+        def _(j):
+            pair = qb_buf[j]
+            kept = lax.div(j * KV_HEADS, ranks)
+            keys, vals = kdup[kept], vdup[kept]
+            outs = []
+            for i in range(2):
+                mine = low if i == 0 else jnp.logical_not(low)
+                query = jnp.where(mine, pair, jnp.zeros_like(pair))
+                scores = lax.dot_general(
+                    query, keys, (((1,), (1,)), ((), ())), preferred_element_type=jnp.float32
+                ) * HEAD_DIM ** (-0.5)
+                masked = jnp.where(allowed, scores, big_negative)
+                sink = tiles[e * ranks + j, groups : groups + 1, i : i + 1]
+                row_max = jnp.maximum(jnp.max(masked, -1, keepdims=True), sink)
+                powers = jnp.exp(masked - row_max)
+                totals = jnp.sum(powers, -1, keepdims=True) + jnp.exp(sink - row_max)
+                probs = (powers / totals).astype(jnp.bfloat16)
+                outs.append(jnp.dot(probs, vals, preferred_element_type=jnp.float32))
+            att[:, pl.ds(pl.multiple_of(j * 128, 128), 128)] = jnp.where(low, outs[0], outs[1]).astype(
+                jnp.bfloat16
+            )
+
+    half_pairs = ranks // 2
+    attend_pairs(0, half_pairs)
 
     def add_in(block, extra):
         block[...] = (block[...].astype(jnp.float32) + extra[...].astype(jnp.float32)).astype(
             jnp.bfloat16
         )
 
-    received(r2_buf.at[1], s2_ss.at[1], s2_rs.at[1])
-    for zz in range(chips):
-        add_in(p_buf.at[e1, zz, c], r2_buf.at[1, zz])
-    send(p_buf.at[e1, :, c], r3_buf, s3_ss.at[0], s3_rs.at[0], (e1, t))
-    received(r2_buf.at[0], s2_ss.at[0], s2_rs.at[0])
-    for zz in range(chips):
-        add_in(p_buf.at[e, zz, c], r2_buf.at[0, zz])
-    if chips > 2:
-        pass_weight(2)
-    received(r3_buf, s3_ss.at[0], s3_rs.at[0])
-    for zz in range(chips):
-        add_in(p_buf.at[e, zz, c], r3_buf.at[zz])
-
-    for k in range(chips - 1):
-        for zz, mine, inner, buf, ss, rs, to in (
-            (chips - 1 - k, z < chips - 1 - k, z > 0, ru_buf, ru_ss, ru_rs, t + 2),
-            (k, z > k, z < chips - 1, rd_buf, rd_ss, rd_rs, t - 2),
-        ):
-
-            @pl.when(mine & inner)
-            def _():
-                received(buf.at[zz], ss.at[zz], rs.at[zz])
-                add_in(p_buf.at[e, zz, c], buf.at[zz])
-
-            send(p_buf.at[e, zz, c], buf.at[zz], ss.at[zz], rs.at[zz], (e, to), mine)
-
+    for n, (zz, when) in enumerate(far_first):
+
+        def second(zz=zz):
+            received(r2_buf.at[1, zz], s2_ss.at[chips + zz], s2_rs.at[chips + zz])
+            add_in(p_buf.at[e1, zz, c], r2_buf.at[1, zz])
+
+        second() if when is None else pl.when(when)(second)
+        send(p_buf.at[e1, zz, c], r3_buf.at[zz], s3_ss.at[zz], s3_rs.at[zz], (e1, t), when)
+        if n % 2:
+            step = (n + 1) // 2
+            attend_pairs(
+                half_pairs + step * half_pairs // (chips + 1),
+                half_pairs + (step + 1) * half_pairs // (chips + 1),
+            )
+
+    for n, (zz, when) in enumerate(far_first):
+
+        def third_sum(zz=zz):
+            received(r2_buf.at[0, zz], s2_ss.at[zz], s2_rs.at[zz])
+            received(r3_buf.at[zz], s3_ss.at[zz], s3_rs.at[zz])
+            block = p_buf.at[e, zz, c]
+            block[...] = (
+                block[...].astype(jnp.float32)
+                + r2_buf[0, zz].astype(jnp.float32)
+                + r3_buf[zz].astype(jnp.float32)
+            ).astype(jnp.bfloat16)
+
+        third_sum() if when is None else pl.when(when)(third_sum)
+        if when is None:
+            continue
+        if n % 2:
+            inner, buf, ss, rs, to = z > 0, ru_buf, ru_ss, ru_rs, t + 2
+        else:
+            inner, buf, ss, rs, to = z < chips - 1, rd_buf, rd_ss, rd_rs, t - 2
+
+        for h in range(2):
+            rows = pl.ds(h * piece_rows, piece_rows)
+            at = zz * 2 + h
+
+            def chain_sum(zz=zz, rows=rows, at=at):
+                received(buf.at[zz, rows, :], ss.at[at], rs.at[at])
+                add_in(p_buf.at[e, zz, c, rows, :], buf.at[zz, rows, :])
+
+            pl.when(when & inner)(chain_sum)
+            send(
+                p_buf.at[e, zz, c, rows, :], buf.at[zz, rows, :], ss.at[at], rs.at[at], (e, to), when
+            )
+
+    attend_pairs(half_pairs + chips * half_pairs // (chips + 1), ranks)
     for k in range(3, chips):
         pass_weight(k)
     for zz in range(chips):
-        received(w_buf.at[zz * 2 + oc], wp_ss.at[zz], wp_rs.at[zz])
+
+        @pl.when(z != zz)
+        def _():
+            received(w_buf.at[zz * 2 + c, taken, :], wx_ss.at[zz], wx_rs.at[zz])
+
+        rest = w_buf.at[zz * 2 + c, taken, :]
+        send(rest, rest, wq_ss.at[zz], wq_rs.at[zz], (e, other), z != zz)
+    for zz in range(chips):
+        received(w_buf.at[zz * 2 + oc, other_carried, :], wp_ss.at[zz], wp_rs.at[zz])
+        received(w_buf.at[zz * 2 + oc, other_taken, :], wq_ss.at[zz], wq_rs.at[zz])
     mix_ref[...] = jnp.dot(
         att[...], w_buf[...].reshape(ranks * 128, width), preferred_element_type=jnp.float32
     ).astype(jnp.bfloat16)
 
     @pl.when(z > 0)
     def _():
-        received(ru_buf.at[z], ru_ss.at[z], ru_rs.at[z])
+        for h in range(2):
+            part = ru_buf.at[z, pl.ds(h * piece_rows, piece_rows), :]
+            received(part, ru_ss.at[z * 2 + h], ru_rs.at[z * 2 + h])
         add_in(p_buf.at[e, z, c], ru_buf.at[z])
 
     @pl.when(z < chips - 1)
     def _():
-        received(rd_buf.at[z], rd_ss.at[z], rd_rs.at[z])
+        for h in range(2):
+            part = rd_buf.at[z, pl.ds(h * piece_rows, piece_rows), :]
+            received(part, rd_ss.at[z * 2 + h], rd_rs.at[z * 2 + h])
         add_in(p_buf.at[e, z, c], rd_buf.at[z])
 
     moe_ref[...] = p_buf[e, z, c]
 
+    pending.extend(weight_copies(z, True, True, None))
+    for k in range(1, chips):
+        pending.extend(weight_copies(jnp.maximum(z - k, 0), True, False, z >= k))
+        pending.extend(
+            weight_copies(jnp.minimum(z + k, chips - 1), False, True, z + k < chips)
+        )
     for when, copy in pending:
         copy.wait_send() if when is None else pl.when(when)(copy.wait_send)
     for slot in range(2 * chips, 4 * chips):
@@ -598,9 +699,9 @@
             p_buf.at[e, :, oc], r1_buf.at[i], s1_ss.at[i], s1_rs.at[i], (e, other)
         ).wait_send()
 
-    for slot in range(2):
+    for place in range(2 * chips):
         remote(
-            p_buf.at[e2, :, c], r2_buf.at[slot], s2_ss.at[slot], s2_rs.at[slot], (e2, t)
+            p_buf.at[e2, 0, c], r2_buf.at[0, 0], s2_ss.at[place], s2_rs.at[place], (e2, t)
         ).wait_send()
 
     @pl.loop(1, ranks)
@@ -647,19 +748,21 @@
         total,
         ranks,
         2,
-        chips,
-        chips,
+        2 * chips,
+        2 * chips,
         4 * chips,
         chips,
         2 * chips,
         chips,
         chips,
         chips,
-        groups,
-        2,
-        1,
         chips,
         chips,
+        groups,
+        2 * chips,
+        chips,
+        2 * chips,
+        2 * chips,
     ):
         sems += [(count,), (count,)]
     block = (row_count, width)
@@ -727,7 +830,7 @@
     groups, ranks = lax.axis_size("ep"), lax.axis_size("tp")
     fits = groups == 4 and ranks % 2 == 0 and ranks <= 8
     fits = fits and queries.shape == (ranks * WINDOW, 2 * HEAD_DIM)
-    fits = fits and key_rows.shape[1] == 128 and moe_rows.shape[0] % 16 == 0
+    fits = fits and key_rows.shape[1] == 128 and moe_rows.shape[0] % 32 == 0
     if fits:
         return fused(
             queries,

time: 113 us -> 89.3 us (0.79)
  Pallas kernels: 106 us -> 83 us
    pallas_call x1, Pallas kernels: 106 us -> 83 us  [fused(): pl.pallas_call(functools.partial(fused_kernel, groups, ranks), out_shape=...]
where the time goes in v3:
time: 89.3 us; the launch traced here: 89.1 us
  Pallas kernels  83 us (93%)
  local copies, waits for them, and re-layouts  3.45 us (4%)
  other arithmetic  1.96 us (2%)
    pallas_call x1, Pallas kernels, fused(): pl.pallas_call(functools.partial(fused_kernel, groups, ranks), out_shape=...  83 us
    unnamed x2, local copies, waits for them, and re-layouts  3.45 us

profile of v3, /device:TPU:0, one launch (start us, length us, event | category | flops | bytes accessed | tf_op | source)
XLA Modules:
  0.0 89.1 jit_solution(17460366181312732818)
XLA Ops:
  0.6 0.7 select_reduce_fusion
  1.3 1.3 %pad_add_fusion.tile_ref = f32[8,128]{1,0:T(8,128)} fusion(f32[1,2]{1,0:T(1,128)} %bitcast.7, f32[4,32]{1,0:T(4,128)S(1)} %select_reduce_fusion), kind=kLoop, calls=%fused_computation | loop fusion | flops 1024 | bytes 4616 | tf_op jit(solution)/shard_map/add | solution.py:742
  2.6 83.0 %shard_map.131 = (bf16[128,2048]{1,0:T(8,128)(2,1)}, bf16[32,2048]{1,0:T(8,128)(2,1)}) custom-call(bf16[1024,128]{1,0:T(8,128)(2,1)} %q_ref.1, bf16[1024,128]{1,0:T(8,128)(2,1)} %key_ref.1, bf16[1024,128]{1,0:T(8,128)(2,1)} %value_ref.1, f32[8,128]{1,0:T(8,128)} %pad_add_fusion.tile_ref, bf16[32,2048]{1,0:T(8,128)(2,1)} %rows_ref.1, f32[1,2048]{1,0:T(1,128)} %bitcast.4, ...), custom_call_target="tpu_custom_call" | custom-call | tf_op jit(solution)/shard_map/pallas_call | solution.py:771
  85.6 1.9 %copy.16 = bf16[128,2048]{1,0:T(8,128)(2,1)} copy(bf16[128,2048]{1,0:T(8,128)(2,1)} %get-tuple-element.4) | data formatting | bytes 1048576
  87.5 1.6 %copy.17 = bf16[32,2048]{1,0:T(8,128)(2,1)} copy(bf16[32,2048]{1,0:T(8,128)(2,1)} %get-tuple-element.5) | data formatting | bytes 262144
